TPU v7x, 32 devices: a whole 2x2x4 slice. The times are simulated.
32 devices in a mesh: gr: 2 (over x), fs: 4 (over z), tp: 4 (over y, core).
Axes of the slice: x: 2, y: 2, z: 4, core: 2. Of those that a mesh axis runs over, the one named last changes fastest.
Arguments:
- tokens: bfloat16 [4096, 2048], P(('gr', 'fs')), may hold values from -6 to 6
- routes: int32 [4096, 2], P(('gr', 'fs')), may hold values from 0 to 3, all different within a row; in each aligned block of 512 rows (0 to 511, 512 to 1023, ...) at most 384 rows name the same one
- route_weight: float32 [4096, 2], P(('gr', 'fs')), may hold values from 0.2 to 1
- gain: float32 [2048], P(('gr', 'fs')), may hold values from 0.1 to 1.9
- w_gate: bfloat16 [4, 2048, 4096], P(None, ('gr', 'fs'), 'tp'), may hold values from -0.125 to 0.125
- w_up: bfloat16 [4, 2048, 4096], P(None, ('gr', 'fs'), 'tp'), may hold values from -0.125 to 0.125
- w_down: bfloat16 [4, 2048, 4096], P(None, ('gr', 'fs'), 'tp'), may hold values from -0.09375 to 0.09375
Outputs:
- gate_out: bfloat16 [4, 2048, 4096], P('fs', None, 'tp')
- up_out: bfloat16 [4, 2048, 4096], P('fs', None, 'tp')
- down_out: bfloat16 [4, 2048, 4096], P('fs', None, 'tp')
- mixed: bfloat16 [4096, 2048], P(('gr', 'fs'), 'tp')
Inputs may be any that keep to these rules, and one draw needn't show every extreme that they name: `routes`: each row names two different experts. Among the 512 rows of one device no expert is named more than 384 times, and in every draw some device names some expert exactly 384 times.
All inputs are finite; a program needn't handle non-finite values.
Results may differ from a plain program's by a relative error of at most 0.015.
Values may be sent and summed in bfloat16 or wider, within the bound.
A program may use at most 128 MiB of HBM per device.

v0:
```python
import jax
import jax.numpy as jnp
from jax import lax
from jax.sharding import PartitionSpec as P

D = 2048
EXP_DEV = 1


EPSILON = 1e-05


def body(tokens, routes, route_weight, gain, w_gate, w_up, w_down):
    scaling = gain[None, :, None]
    gate_local = (w_gate * scaling).astype(jnp.bfloat16)
    up_local = (w_up * scaling).astype(jnp.bfloat16)
    gate_mine, up_mine, down_mine = (
        lax.all_to_all(gate_local, "fs", split_axis=0, concat_axis=1, tiled=True),
        lax.all_to_all(up_local, "fs", split_axis=0, concat_axis=1, tiled=True),
        lax.all_to_all(w_down, "fs", split_axis=0, concat_axis=1, tiled=True),
    )
    gate_out, up_out, down_out = (
        lax.all_gather(gate_mine, "gr", axis=1, tiled=True),
        lax.all_gather(up_mine, "gr", axis=1, tiled=True),
        lax.all_gather(down_mine, "gr", axis=1, tiled=True),
    )
    fs_count = lax.axis_size("fs")
    experts = EXP_DEV * fs_count
    tok_rows = tokens.shape[0]
    capacity = 3 * tok_rows // experts
    float_rows = tokens.astype(jnp.float32)
    normed = (
        float_rows * lax.rsqrt(jnp.mean(float_rows * float_rows, axis=-1, keepdims=True) + EPSILON)
    ).astype(jnp.bfloat16)
    flat_ids = routes.reshape(-1)
    onehot = (flat_ids[:, None] == jnp.arange(experts, dtype=jnp.int32)[None, :]).astype(jnp.int32)
    slot_rank = jnp.sum((jnp.cumsum(onehot, axis=0) - onehot) * onehot, axis=-1)
    destination = (flat_ids * capacity + slot_rank).reshape(tok_rows, 2)
    slot_ids = jnp.arange(experts * capacity, dtype=jnp.int32)
    hits = slot_ids[:, None, None] == destination[None, :, :]
    dispatch = jnp.any(hits, axis=-1).astype(jnp.bfloat16)
    outgoing = jnp.dot(dispatch, normed, preferred_element_type=jnp.float32).astype(jnp.bfloat16)
    outgoing = outgoing.reshape(fs_count, EXP_DEV, capacity, D)
    arrived = lax.all_to_all(outgoing, "fs", split_axis=0, concat_axis=0, tiled=True)
    gate = jnp.einsum("sjnd,jdf->sjnf", arrived, gate_out, preferred_element_type=jnp.float32)
    upper = jnp.einsum("sjnd,jdf->sjnf", arrived, up_out, preferred_element_type=jnp.float32)
    hidden = (jax.nn.silu(gate) * upper).astype(jnp.bfloat16)
    partial_value = jnp.einsum(
        "sjnf,jdf->sjnd", hidden, down_out, preferred_element_type=jnp.float32
    )
    rounded = lax.optimization_barrier(partial_value.astype(jnp.bfloat16))
    summed = lax.psum_scatter(
        rounded.astype(jnp.float32).astype(jnp.bfloat16), "tp", scatter_dimension=3, tiled=True
    )
    back_home = lax.all_to_all(summed, "fs", split_axis=0, concat_axis=0, tiled=True)
    features = back_home.shape[-1]
    flat_back = back_home.reshape(experts * capacity, features).astype(jnp.float32)
    first = jnp.where(slot_ids[None, :] == destination[:, 0:1], route_weight[:, 0:1], 0.0)
    second = jnp.where(slot_ids[None, :] == destination[:, 1:2], route_weight[:, 1:2], 0.0)
    combine_map = first + second
    mixed = jnp.dot(
        combine_map, flat_back, precision=lax.Precision.HIGHEST, preferred_element_type=jnp.float32
    ).astype(jnp.bfloat16)
    return (gate_out, up_out, down_out, mixed)


def solution(mesh):
    in_specs = (
        P(("gr", "fs"), None),
        P(("gr", "fs"), None),
        P(("gr", "fs"), None),
        P(("gr", "fs")),
        P(None, ("gr", "fs"), "tp"),
        P(None, ("gr", "fs"), "tp"),
        P(None, ("gr", "fs"), "tp"),
    )
    out_specs = (
        P("fs", None, "tp"),
        P("fs", None, "tp"),
        P("fs", None, "tp"),
        P(("gr", "fs"), "tp"),
    )
    return jax.shard_map(body, mesh=mesh, in_specs=in_specs, out_specs=out_specs, check_vma=False)
```

profile of v0, /device:TPU:4, one launch (start us, length us, event | category | flops | bytes accessed | tf_op | source)
XLA Modules:
  0.0 454.6 jit_solution(13460265644563820947)
XLA Ops:
  7.2 3.7 multiply_convert_fusion
  10.9 53.0 %all_to_all.46 = bf16[4,256,1024]{2,1,0:T(8,128)(2,1)} all-to-all(bf16[4,256,1024]{2,1,0:T(8,128)(2,1)S(1)} %get-tuple-element.32), channel_id=1, replica_groups=mesh['gr'=2,'fs'=4,'tp'=4] {'fs'}, dimensions={0} | all-to-all | bytes 4194304 | tf_op jit(solution)/shard_map/all_to_all | solution.py:19
  63.9 50.8 %all_to_all.47 = bf16[4,256,1024]{2,1,0:T(8,128)(2,1)} all-to-all(bf16[4,256,1024]{2,1,0:T(8,128)(2,1)S(1)} %get-tuple-element.33), channel_id=1, replica_groups=mesh['gr'=2,'fs'=4,'tp'=4] {'fs'}, dimensions={0} | all-to-all | bytes 4194304 | tf_op jit(solution)/shard_map/all_to_all | solution.py:18
  114.6 3.6 all-to-all-start.2
  118.3 0.1 copy.60
  118.5 0.2 eq.73
  118.6 1.1 reduce-window.6
  119.8 0.2 slice_reduce_fusion
  120.0 0.2 reduce-window.9
  120.2 3.9 copy.70
  124.2 0.2 eq.69
  124.4 0.2 reduce_sum.21
  124.8 2.0 fusion.8
  126.8 2.1 fusion.9
  128.8 7.1 %convolution_convert_fusion = bf16[1536,2048]{1,0:T(8,128)(2,1)} fusion(pred[1536,512]{1,0:T(8,128)(4,1)S(1)} %fusion.8, bf16[512,2048]{1,0:T(8,128)(2,1)} %param.7, f32[512]{0:T(512)S(1)} %add_rsqrt_fusion), kind=kOutput, calls=%fused_computation | convolution fusion | flops 3227516928 | bytes 9177088 | tf_op jit(solution)/shard_map/dot_general | solution.py:42
  135.9 29.5 %all-to-all-done.2 = bf16[4,256,1024]{2,1,0:T(8,128)(2,1)S(1)} async-done(((bf16[4,256,1024]{2,1,0:T(8,128)(2,1)}), bf16[4,256,1024]{2,1,0:T(8,128)(2,1)S(1)}, u32[]{:S(2)}, u32[]{:S(2)}) %all-to-all-start.2) | async-done | bytes 2097184 | tf_op jit(solution)/shard_map/all_to_all | solution.py:20
  165.4 1.3 copy-done
  166.7 5.2 %all-to-all-start.3 = ((bf16[4,1,384,2048]{3,2,1,0:T(8,128)(2,1)}), bf16[4,1,384,2048]{3,2,1,0:T(8,128)(2,1)}, u32[]{:S(2)}, u32[]{:S(2)}) async-start(bf16[4,1,384,2048]{3,2,1,0:T(8,128)(2,1)} %bitcast.103), calls=%async_computation.3 | async-start | bytes 12582912 | tf_op jit(solution)/shard_map/all_to_all | solution.py:44
  172.1 3.9 copy.69
  176.1 0.7 all-gather.8.cloned.1.call-update
  176.8 0.2 reduce-scatter.2.cloned.1.call-start
  177.0 5.4 %all-gather.6.cloned.1.call-done = bf16[1,2048,1024]{1,2,0:T(8,128)(2,1)} async-done(((bf16[1,1024,1024]{1,2,0:T(8,128)(2,1)}), bf16[1,2048,1024]{1,2,0:T(8,128)(2,1)}) %all-gather.6.cloned.1.call-update) | async-done | bytes 4194320 | tf_op jit(solution)/shard_map/all_gather | solution.py:24
  182.4 127.3 %all-to-all-done.3 = bf16[4,1,384,2048]{3,2,1,0:T(8,128)(2,1)} async-done(((bf16[4,1,384,2048]{3,2,1,0:T(8,128)(2,1)}), bf16[4,1,384,2048]{3,2,1,0:T(8,128)(2,1)}, u32[]{:S(2)}, u32[]{:S(2)}) %all-to-all-start.3) | async-done | bytes 6291488 | tf_op jit(solution)/shard_map/all_to_all | solution.py:44
  309.7 11.7 %fusion.4 = f32[1024,4,384]{2,0,1:T(8,128)} fusion(bf16[4,1,384,2048]{3,2,1,0:T(8,128)(2,1)} %all-to-all-done.3, bf16[1,2048,1024]{1,2,0:T(8,128)(2,1)} %all-gather.6.cloned.1.call-done), kind=kOutput, calls=%fused_computation.8 | convolution fusion | flops 6442450944 | bytes 16777216 | tf_op jit(solution)/shard_map/sjnd,jdf->sjnf/dot_general | solution.py:46
  321.4 23.3 %convert_bitcast_fusion = bf16[4,1,384,2048]{3,2,0,1:T(8,128)(2,1)} fusion(bf16[1,2048,1024]{2,1,0:T(8,128)(2,1)} %all-gather.8.cloned.1.call-done, f32[1024,4,384]{2,0,1:T(8,128)} %fusion.4, bf16[4,1,384,2048]{3,2,1,0:T(8,128)(2,1)} %all-to-all-done.3, bf16[1,2048,1024]{1,2,0:T(8,128)(2,1)} %all-gather.4.cloned.1.call-done), kind=kOutput, calls=%fused_computation.12 | convolution fusion | flops 12897484800 | bytes 27262976 | tf_op jit(solution)/shard_map/sjnf,jdf->sjnd/dot_general | solution.py:48
  344.7 55.9 %reduce-scatter.2.cloned.1.call-done = bf16[4,1,384,512]{3,2,0,1:T(8,128)(2,1)} async-done(((bf16[4,1,384,2048]{3,2,0,1:T(8,128)(2,1)}), bf16[4,1,384,512]{3,2,0,1:T(8,128)(2,1)}) %reduce-scatter.2.cloned.1.call-update) | async-done | bytes 1572880 | tf_op jit(solution)/shard_map/reduce_scatter | solution.py:52
  400.6 4.8 %all-to-all-start.4 = ((bf16[4,1,384,512]{3,2,1,0:T(8,128)(2,1)}), bf16[4,1,384,512]{3,2,1,0:T(8,128)(2,1)S(1)}, u32[]{:S(2)}, u32[]{:S(2)}) async-start(bf16[4,1,384,512]{3,2,1,0:T(8,128)(2,1)} %bitcast.104), calls=%async_computation.5 | async-start | bytes 3145728 | tf_op jit(solution)/shard_map/all_to_all | solution.py:55
  405.5 6.4 %copy.66 = bf16[1,2048,1024]{2,1,0:T(8,128)(2,1)} copy(bf16[1,2048,1024]{1,2,0:T(8,128)(2,1)} %all-gather.4.cloned.1.call-done) | data formatting | bytes 8388608
  411.9 6.4 %copy.67 = bf16[1,2048,1024]{2,1,0:T(8,128)(2,1)} copy(bf16[1,2048,1024]{1,2,0:T(8,128)(2,1)} %all-gather.6.cloned.1.call-done) | data formatting | bytes 8388608
  418.3 24.0 %all-to-all-done.4 = bf16[4,1,384,512]{3,2,1,0:T(8,128)(2,1)S(1)} async-done(((bf16[4,1,384,512]{3,2,1,0:T(8,128)(2,1)}), bf16[4,1,384,512]{3,2,1,0:T(8,128)(2,1)S(1)}, u32[]{:S(2)}, u32[]{:S(2)}) %all-to-all-start.4) | async-done | bytes 1572896 | tf_op jit(solution)/shard_map/all_to_all | solution.py:55
  442.2 3.8 fusion.38
  446.1 2.0 copy.74
  (23 shorter events, 0.4 us)
Async XLA Ops:
  63.9 54.4 %copy-start.2 = (s32[512,2]{0,1:T(2,128)S(1)}, s32[512,2]{0,1:T(2,128)}, u32[]{:S(2)}) copy-start(s32[512,2]{0,1:T(2,128)} %param.8) | copy-start | bytes 12292
  114.6 50.8 %all-to-all-start.2 = ((bf16[4,256,1024]{2,1,0:T(8,128)(2,1)}), bf16[4,256,1024]{2,1,0:T(8,128)(2,1)S(1)}, u32[]{:S(2)}, u32[]{:S(2)}) async-start(bf16[4,256,1024]{2,1,0:T(8,128)(2,1)} %param.13), calls=%async_computation.2 | async-start | bytes 4194304 | tf_op jit(solution)/shard_map/all_to_all | solution.py:20
  118.3 64.1 %all-gather.6.cloned.1.call-start = ((), (), s32[]{:S(2)}) async-start(), calls=%async_computation.7 | async-start | bytes 6291456 | tf_op jit(solution)/shard_map/all_gather | solution.py:24
  165.4 1.3 copy-start
  166.7 143.0 %all-to-all-start.3 = ((bf16[4,1,384,2048]{3,2,1,0:T(8,128)(2,1)}), bf16[4,1,384,2048]{3,2,1,0:T(8,128)(2,1)}, u32[]{:S(2)}, u32[]{:S(2)}) async-start(bf16[4,1,384,2048]{3,2,1,0:T(8,128)(2,1)} %bitcast.103), calls=%async_computation.3 | async-start | bytes 12582912 | tf_op jit(solution)/shard_map/all_to_all | solution.py:44
  172.0 149.4 %all-gather.4.cloned.1.call-start = ((), (), s32[]{:S(2)}) async-start(), calls=%async_computation.6 | async-start | bytes 6291456 | tf_op jit(solution)/shard_map/all_gather | solution.py:23
  176.0 145.4 %all-gather.8.cloned.1.call-start = ((), (), s32[]{:S(2)}) async-start(), calls=%async_computation.8 | async-start | bytes 6291456 | tf_op jit(solution)/shard_map/all_gather | solution.py:25
  176.8 223.9 %reduce-scatter.2.cloned.1.call-start = ((), (), s32[]{:S(2)}) async-start(), calls=%async_computation.9 | async-start | bytes 7864320 | tf_op jit(solution)/shard_map/reduce_scatter | solution.py:52
  344.7 60.8 %copy-start.3 = (f32[512,2]{0,1:T(2,128)S(1)}, f32[512,2]{0,1:T(2,128)}, u32[]{:S(2)}) copy-start(f32[512,2]{0,1:T(2,128)} %param.9) | copy-start | bytes 12292
  400.6 41.6 %all-to-all-start.4 = ((bf16[4,1,384,512]{3,2,1,0:T(8,128)(2,1)}), bf16[4,1,384,512]{3,2,1,0:T(8,128)(2,1)S(1)}, u32[]{:S(2)}, u32[]{:S(2)}) async-start(bf16[4,1,384,512]{3,2,1,0:T(8,128)(2,1)} %bitcast.104), calls=%async_computation.5 | async-start | bytes 3145728 | tf_op jit(solution)/shard_map/all_to_all | solution.py:55
  442.2 3.8 copy-start.1
Sparse Core Ops, SparseCore 0:
  124.3 58.0 all-gather.5
  184.5 56.7 all-gather.3
  243.4 56.7 all-gather.7
  344.8 55.7 reduce-scatter.1
where the time goes:
time: 458 us; the launch traced here: 455 us
  waiting for transfers between devices  243 us (53%)
  blocking collectives  104 us (23%)
  matrix products  45.8 us (10%)
  local copies, waits for them, and re-layouts  25 us (5%)
  starting transfers between devices  14 us (3%)
  between operations  13.9 us (3%)
  other arithmetic  9.24 us (2%)
    all_to_all x1, waiting for transfers between devices, body(): lax.all_to_all(outgoing, 'fs', split_axis=0, concat_axis=0, tiled=True)  127 us
    reduce_scatter x1, waiting for transfers between devices, body(): lax.psum_scatter(rounded.astype(jnp.float32).astype(jnp.bfloat16), 'tp',...  55.9 us
    all_to_all x1, blocking collectives, body(): lax.all_to_all(up_local, 'fs', split_axis=0, concat_axis=1, tiled=True)  53 us
    all_to_all x1, blocking collectives, body(): lax.all_to_all(gate_local, 'fs', split_axis=0, concat_axis=1, tiled=True)  50.8 us
    all_to_all x1, waiting for transfers between devices, body(): lax.all_to_all(w_down, 'fs', split_axis=0, concat_axis=1, tiled=True)  29.5 us
    all_to_all x1, waiting for transfers between devices, body(): lax.all_to_all(summed, 'fs', split_axis=0, concat_axis=0, tiled=True)  24 us
    dot_general x1, matrix products, body(): jnp.einsum('sjnf,jdf->sjnd', hidden, down_out, preferred_element_type=jnp...  23.3 us
    unnamed x12, local copies, waits for them, and re-layouts  16.3 us
  transfers between devices with their start and end apart: 7, of which 5 were waited for; matrix products, arithmetic and copies ran while one was open for 10% of the time, Pallas kernels for 0%

commit v1 on v0

--- a/solution.py
+++ b/solution.py
@@ -1,9 +1,276 @@
+import functools
 import jax
 import jax.numpy as jnp
 from jax import lax
+from jax.experimental import pallas as pl
+from jax.experimental.pallas import tpu as pltpu
 from jax.sharding import PartitionSpec as P
 
-D = 2048
+MESH = pl.DeviceIdType.MESH
+VMEM_LIMIT = 66 * 1000 * 1000
+
+
+def kernel(ng, nz, nt, tok_in, wt, gw, uw, dw, gout, uout, dout, mixed,
+           tok, hid, part, crx, yrx, ret,
+           ts, tr, fs_s, fr, ws, wr, xs, xr, cs, cr, ys, yr, rs, rr):
+    g, z, t = lax.axis_index("gr"), lax.axis_index("fs"), lax.axis_index("tp")
+    core, y = lax.rem(t, 2), lax.div(t, 2)
+    rows, quarter = tok_in.shape[1], tok_in.shape[2]
+    chunk, width = gw.shape[1], gw.shape[2]
+    chunks = ng * nz
+    per_owner = chunks // nt
+    srcs = (gw, uw, dw)
+    outs = (gout, uout, dout)
+    ks = sorted(range(1, nz), key=lambda k: min(k, nz - k))
+
+    def to(k):
+        return lax.rem(z + k, nz)
+
+    def frm(k):
+        return lax.rem(z + nz - k, nz)
+
+    def rdma(src, dst, ss, rsem, dev):
+        return pltpu.make_async_remote_copy(
+            src_ref=src, dst_ref=dst, send_sem=ss, recv_sem=rsem, device_id=dev, device_id_type=MESH
+        )
+
+    def rows_of(m, group, zs):
+        return outs[m].at[pl.ds(pl.multiple_of((group * nz + zs) * chunk, chunk), chunk), :]
+
+    barrier = pltpu.get_barrier_semaphore()
+    for k in range(1, nz):
+        pl.semaphore_signal(barrier, inc=1, device_id={"fs": to(k)}, device_id_type=MESH)
+    for j in range(1, nt):
+        pl.semaphore_signal(barrier, inc=1, device_id={"tp": lax.rem(t + j, nt)}, device_id_type=MESH)
+    pl.semaphore_signal(barrier, inc=1, device_id={"gr": 1 - g}, device_id_type=MESH)
+    pl.semaphore_wait(barrier, nz + nt - 1)
+
+    sends = []
+
+    def z_send(m, k):
+        c = rdma(srcs[m].at[to(k)], rows_of(m, g, z), ws.at[m, k], wr.at[m, k], {"fs": to(k)})
+        c.start()
+        sends.append(c)
+
+    def x_send(m, k, src):
+        c = rdma(src, rows_of(m, g, frm(k)), xs.at[m, k], xr.at[m, k], {"gr": 1 - g})
+        c.start()
+        sends.append(c)
+
+    def z_take(m, k):
+        ref = rows_of(m, g, frm(k))
+        rdma(ref, ref, ws.at[m, k], wr.at[m, k], {"fs": to(k)}).wait_recv()
+        x_send(m, k, ref)
+
+    def x_take(m, k):
+        ref = rows_of(m, 1 - g, frm(k))
+        rdma(ref, ref, xs.at[m, k], xr.at[m, k], {"gr": 1 - g}).wait_recv()
+
+    for m in range(3):
+        x_send(m, 0, srcs[m].at[z])
+    for k in ks:
+        c = rdma(tok_in.at[t], tok.at[t, z], ts.at[k], tr.at[k], {"fs": to(k)})
+        c.start()
+        sends.append(c)
+    for m in range(2):
+        for k in ks:
+            z_send(m, k)
+    for m in range(3):
+        outs[m][pl.ds(pl.multiple_of((g * nz + z) * chunk, chunk), chunk), :] = srcs[m][z]
+    for q in range(nt):
+        tok[q, z] = tok_in[q]
+    for k in ks:
+        ref = tok.at[t, frm(k)]
+        rdma(ref, ref, ts.at[k], tr.at[k], {"fs": to(k)}).wait_recv()
+        for j in range(1, nt):
+            c = rdma(ref, ref, fs_s.at[j, k], fr.at[j, k], {"tp": lax.rem(t + j, nt)})
+            c.start()
+            sends.append(c)
+    for k in ks:
+        z_send(2, k)
+    for m in range(2):
+        for k in ks:
+            z_take(m, k)
+    for k in ks:
+        for j in range(1, nt):
+            ref = tok.at[lax.rem(t + nt - j, nt), frm(k)]
+            rdma(ref, ref, fs_s.at[j, k], fr.at[j, k], {"tp": lax.rem(t + j, nt)}).wait_recv()
+    for m in range(2):
+        for k in [0] + ks:
+            x_take(m, k)
+
+    tile = 256
+    tiles = width // tile
+
+    def hidden(lo, hi):
+        @pl.loop(lo * tiles, hi * tiles)
+        def _(i):
+            b = i // tiles
+            cols = pl.ds(pl.multiple_of((i % tiles) * tile, tile), tile)
+            gate = jnp.zeros((rows, tile), jnp.float32)
+            upper = jnp.zeros((rows, tile), jnp.float32)
+            for q in range(nt):
+                a = tok[q, b]
+                gate += jnp.dot(a, gout[q * quarter:(q + 1) * quarter, cols], preferred_element_type=jnp.float32)
+                upper += jnp.dot(a, uout[q * quarter:(q + 1) * quarter, cols], preferred_element_type=jnp.float32)
+            hid[b, :, cols] = (gate / (1.0 + jnp.exp(-gate)) * upper).astype(jnp.bfloat16)
+
+    cuts = [nz * (i + 1) // nz for i in range(nz)]
+    late = list(ks)
+    done = 0
+    for i, hi in enumerate(cuts):
+        hidden(done, hi)
+        done = hi
+        if i >= 1 and len(late) > 1:
+            z_take(2, late.pop(0))
+
+    def ids(c):
+        owner = c // per_owner
+        return owner, lax.rem(owner, 2), lax.div(owner, 2), lax.rem(c, per_owner)
+
+    finals = []
+
+    def stage_a(i, c):
+        mine = pl.ds(pl.multiple_of(c * chunk, chunk), chunk)
+
+        @pl.loop(0, nz)
+        def _(b):
+            part[c, b] = lax.dot_general(
+                hid[b], dout[mine, :], (((1,), (1,)), ((), ())), preferred_element_type=jnp.float32
+            ).astype(jnp.bfloat16)
+
+        owner, par, yo, cc = ids(c)
+        give = rdma(part.at[c], crx.at[yo * per_owner + cc], cs.at[i], cr.at[i], {"tp": y * 2 + 1 - core})
+
+        @pl.when(par != core)
+        def _():
+            give.start()
+        finals.append((par != core, give))
+
+    def stage_b(i, c):
+        owner, par, yo, cc = ids(c)
+        up = rdma(part.at[c], yrx.at[cc], ys.at[i], yr.at[i], {"tp": yo * 2 + core})
+        away = jnp.logical_and(par == core, yo != y)
+
+        @pl.when(par == core)
+        def _():
+            slot = crx.at[yo * per_owner + cc]
+            rdma(slot, slot, cs.at[i], cr.at[i], {"tp": y * 2 + 1 - core}).wait_recv()
+
+            @pl.loop(0, nz)
+            def _(b):
+                part[c, b] = (
+                    part[c, b].astype(jnp.float32) + crx[yo * per_owner + cc, b].astype(jnp.float32)
+                ).astype(jnp.bfloat16)
+
+        @pl.when(away)
+        def _():
+            up.start()
+        finals.append((away, up))
+
+    def stage_c(i, c):
+        owner, par, yo, cc = ids(c)
+        home = [
+            rdma(part.at[c, to(k)], ret.at[z, cc], rs.at[k, cc], rr.at[k, cc], {"fs": to(k)}) for k in ks
+        ]
+
+        @pl.when(owner == t)
+        def _():
+            slot = yrx.at[cc]
+            rdma(slot, slot, ys.at[i], yr.at[i], {"tp": (1 - y) * 2 + core}).wait_recv()
+
+            @pl.loop(0, nz)
+            def _(b):
+                part[c, b] = (
+                    part[c, b].astype(jnp.float32) + yrx[cc, b].astype(jnp.float32)
+                ).astype(jnp.bfloat16)
+            for h in home:
+                h.start()
+            ret[z, cc] = part[c, z]
+        for h in home:
+            finals.append((owner == t, h))
+
+    order = [(0, 0), (1, 0)] + [(0, k) for k in ks] + [(1, k) for k in ks]
+    seq = [((g if side == 0 else 1 - g) * nz + frm(k), side, k) for side, k in order]
+    n = len(seq)
+    for i in range(n + 2):
+        if i < n:
+            c, side, k = seq[i]
+            if side == 1:
+                x_take(2, k)
+            elif k in late:
+                z_take(2, k)
+                late.remove(k)
+            stage_a(i, c)
+        if 0 <= i - 1 < n:
+            stage_b(i - 1, seq[i - 1][0])
+        if 0 <= i - 2 < n:
+            stage_c(i - 2, seq[i - 2][0])
+
+    for k in ks:
+        for cc in range(per_owner):
+            ref = ret.at[frm(k), cc]
+            rdma(ref, ref, rs.at[k, cc], rr.at[k, cc], {"fs": to(k)}).wait_recv()
+    for cc in range(per_owner):
+        total = wt[:, 0:1] * ret[0, cc].astype(jnp.float32)
+        for e in range(1, nz):
+            total += wt[:, e:e + 1] * ret[e, cc].astype(jnp.float32)
+        mixed[:, cc * chunk:(cc + 1) * chunk] = total.astype(jnp.bfloat16)
+    for c in sends:
+        c.wait_send()
+    for flag, c in finals:
+        @pl.when(flag)
+        def _(c=c):
+            c.wait_send()
+
+
+def fused(ng, nz, nt, tokens, routes, route_weight, gain, w_gate, w_up, w_down):
+    scaling = gain[None, :, None]
+    gate_local = (w_gate * scaling).astype(jnp.bfloat16)
+    up_local = (w_up * scaling).astype(jnp.bfloat16)
+    rows, d = tokens.shape
+    quarter = d // nt
+    experts, chunk, width = w_gate.shape
+    chunks = ng * nz
+    per_owner = chunks // nt
+    float_rows = tokens.astype(jnp.float32)
+    normed = (
+        float_rows * lax.rsqrt(jnp.mean(float_rows * float_rows, axis=-1, keepdims=True) + EPSILON)
+    ).astype(jnp.bfloat16)
+    normed = normed.reshape(rows, nt, quarter).transpose(1, 0, 2)
+    ids = jnp.arange(experts, dtype=jnp.int32)
+    wt = jnp.sum(jnp.where(routes[:, :, None] == ids, route_weight[:, :, None], 0.0), axis=1)
+    bf = jnp.bfloat16
+    dma = pltpu.SemaphoreType.DMA
+    full = jax.ShapeDtypeStruct((d, width), bf)
+    vmem = pl.BlockSpec(memory_space=pltpu.VMEM)
+    outs = pl.pallas_call(
+        functools.partial(kernel, ng, nz, nt),
+        out_shape=(full, full, full, jax.ShapeDtypeStruct((rows, quarter), bf)),
+        in_specs=[vmem] * 5,
+        out_specs=(vmem,) * 4,
+        scratch_shapes=[
+            pltpu.VMEM((nt, nz, rows, quarter), bf),
+            pltpu.VMEM((nz, rows, width), bf),
+            pltpu.VMEM((chunks, nz, rows, chunk), bf),
+            pltpu.VMEM((chunks // 2, nz, rows, chunk), bf),
+            pltpu.VMEM((per_owner, nz, rows, chunk), bf),
+            pltpu.VMEM((nz, per_owner, rows, chunk), bf),
+            dma((nz,)), dma((nz,)),
+            dma((nt, nz)), dma((nt, nz)),
+            dma((3, nz)), dma((3, nz)),
+            dma((3, nz)), dma((3, nz)),
+            dma((chunks,)), dma((chunks,)),
+            dma((chunks,)), dma((chunks,)),
+            dma((nz, per_owner)), dma((nz, per_owner)),
+        ],
+        compiler_params=pltpu.CompilerParams(
+            collective_id=0, has_side_effects=True, vmem_limit_bytes=VMEM_LIMIT
+        ),
+    )(normed, wt, gate_local, up_local, w_down)
+    gate_out, up_out, down_out, mixed = outs
+    return (gate_out[None], up_out[None], down_out[None], mixed)
+
 EXP_DEV = 1
 
 
@@ -40,7 +307,7 @@
     hits = slot_ids[:, None, None] == destination[None, :, :]
     dispatch = jnp.any(hits, axis=-1).astype(jnp.bfloat16)
     outgoing = jnp.dot(dispatch, normed, preferred_element_type=jnp.float32).astype(jnp.bfloat16)
-    outgoing = outgoing.reshape(fs_count, EXP_DEV, capacity, D)
+    outgoing = outgoing.reshape(fs_count, EXP_DEV, capacity, tokens.shape[1])
     arrived = lax.all_to_all(outgoing, "fs", split_axis=0, concat_axis=0, tiled=True)
     gate = jnp.einsum("sjnd,jdf->sjnf", arrived, gate_out, preferred_element_type=jnp.float32)
     upper = jnp.einsum("sjnd,jdf->sjnf", arrived, up_out, preferred_element_type=jnp.float32)
@@ -80,4 +347,7 @@
         P("fs", None, "tp"),
         P(("gr", "fs"), "tp"),
     )
-    return jax.shard_map(body, mesh=mesh, in_specs=in_specs, out_specs=out_specs, check_vma=False)
+    ng, nz, nt = mesh.shape["gr"], mesh.shape["fs"], mesh.shape["tp"]
+    small = ng == 2 and nt == 4 and nz <= 4
+    work = functools.partial(fused, ng, nz, nt) if small else body
+    return jax.shard_map(work, mesh=mesh, in_specs=in_specs, out_specs=out_specs, check_vma=False)

time: 458 us -> 339 us (0.74)
  Pallas kernels: 0 us -> 310 us
  waiting for transfers between devices: 243 us -> 0 us
  blocking collectives: 104 us -> 0 us
  matrix products: 45.8 us -> 0 us
  starting transfers between devices: 14 us -> 0 us
  between operations: 13.9 us -> 0.67 us
  local copies, waits for them, and re-layouts: 25 us -> 19.3 us
    pallas_call x0 -> x1, Pallas kernels: none -> 310 us  [fused(): pl.pallas_call(functools.partial(kernel, ng, nz, nt), out_shape=(full, fu...]
    all_to_all x3 -> x0, waiting for transfers between devices: 181 us -> none  [the longest x1 127 us: body(): lax.all_to_all(outgoing, 'fs', split_axis=0, concat_axis=0, tiled=True)]
    all_to_all x2 -> x0, blocking collectives: 104 us -> none  [the longest x1 53 us: body(): lax.all_to_all(up_local, 'fs', split_axis=0, concat_axis=1, tiled=True)]
    reduce_scatter x1 -> x0, waiting for transfers between devices: 55.9 us -> none  [body(): lax.psum_scatter(rounded.astype(jnp.float32).astype(jnp.bfloat16), 'tp',...]
    dot_general x4 -> x0, matrix products: 45.8 us -> none  [the longest x1 23.3 us: body(): jnp.einsum('sjnf,jdf->sjnd', hidden, down_out, preferred_element_type=jnp...]
    all_to_all x3 -> x0, starting transfers between devices: 13.7 us -> none  [the longest x1 5.25 us: body(): lax.all_to_all(outgoing, 'fs', split_axis=0, concat_axis=0, tiled=True)]
    all_to_all x2 -> x0, local copies, waits for them, and re-layouts: 7.88 us -> none  [the longest x1 3.94 us: body(): lax.all_to_all(gate_local, 'fs', split_axis=0, concat_axis=1, tiled=True)]
    all_gather x3 -> x0, waiting for transfers between devices: 5.39 us -> none  [the longest x1 5.39 us: body(): lax.all_gather(up_mine, 'gr', axis=1, tiled=True)]
  transfers between devices with their start and end apart: 7 -> 0, of which waited for: 5 -> 0; matrix products, arithmetic and copies ran while one was open for 10% -> 0% of each run, Pallas kernels for 0% -> 0%
where the time goes in v1:
time: 339 us; the launch traced here: 338 us
  Pallas kernels  310 us (91%)
  local copies, waits for them, and re-layouts  19.3 us (6%)
  other arithmetic  8.15 us (2%)
    pallas_call x1, Pallas kernels, fused(): pl.pallas_call(functools.partial(kernel, ng, nz, nt), out_shape=(full, fu...  310 us
    unnamed x15, local copies, waits for them, and re-layouts  14.2 us

profile of v1, /device:TPU:4, one launch (start us, length us, event | category | flops | bytes accessed | tf_op | source)
XLA Modules:
  0.0 338.5 jit_solution(15256828196737941906)
XLA Ops:
  0.6 0.7 select_reduce_fusion
  1.4 0.9 copy.19.wt
  2.2 2.9 copy.17
  5.1 0.5 fusion
  5.6 0.0 copy-start.4
  5.6 1.8 fusion.1
  7.4 0.0 copy-start.2
  7.4 4.3 %copy.18 = bf16[512,4,512]{2,0,1:T(8,128)(2,1)} copy(bf16[512,4,512]{0,2,1:T(8,128)(2,1)} %bitcast.5) | data formatting | bytes 4194304 | tf_op jit(solution)/shard_map/reshape | solution.py:240
  11.7 0.0 copy-done.4
  11.7 0.0 copy-done.2
  11.7 5.2 %multiply_convert_fusion = (bf16[4,256,1024]{2,1,0:T(8,128)(2,1)}, bf16[4,256,1024]{2,1,0:T(8,128)(2,1)}) fusion(bf16[4,256,1024]{2,1,0:T(8,128)(2,1)S(1)} %copy-done.2, f32[256]{0:T(256)S(1)} %copy-done.4, bf16[4,256,1024]{2,1,0:T(8,128)(2,1)} %param.11), kind=kLoop, calls=%fused_computation.4 | loop fusion | flops 6291456 | bytes 8389632 | tf_op jit(solution)/shard_map/convert_element_type | solution.py:230
  16.8 310.3 %shard_map.102 = (bf16[2048,1024]{1,0:T(8,128)(2,1)}, bf16[2048,1024]{1,0:T(8,128)(2,1)}, bf16[2048,1024]{1,0:T(8,128)(2,1)}, bf16[512,512]{1,0:T(8,128)(2,1)}) custom-call(bf16[4,512,512]{2,1,0:T(8,128)(2,1)} %bitcast.6, f32[512,4]{1,0:T(8,128)} %copy.19.wt, bf16[4,256,1024]{2,1,0:T(8,128)(2,1)} %get-tuple-element.13.gw, ...), custom_call_target="tpu_custom_call" | custom-call | tf_op jit(solution)/shard_map/pallas_call | solution.py:247
  327.1 0.0 copy-start.1
  327.1 4.8 %copy.24 = bf16[1,2048,1024]{2,1,0:T(8,128)(2,1)} copy(bf16[1,2048,1024]{2,1,0:T(8,128)(2,1)} %bitcast.9) | data formatting | bytes 8388608
  331.9 0.0 copy-done.1
  331.9 0.0 copy-start
  331.9 2.1 copy.25
  334.1 1.6 copy-done
  335.6 0.0 copy-start.3
  335.6 2.0 copy.26
  337.7 0.0 copy-done.3
  337.7 0.8 copy.27
  (1 shorter events, 0.0 us)
Async XLA Ops:
  5.6 6.1 %copy-start.4 = (f32[256]{0:T(256)S(1)}, f32[256]{0:T(256)}, u32[]{:S(2)}) copy-start(f32[256]{0:T(256)} %param.10) | copy-start | bytes 3076
  7.4 4.3 %copy-start.2 = (bf16[4,256,1024]{2,1,0:T(8,128)(2,1)S(1)}, bf16[4,256,1024]{2,1,0:T(8,128)(2,1)}, u32[]{:S(2)}) copy-start(bf16[4,256,1024]{2,1,0:T(8,128)(2,1)} %param.12) | copy-start | bytes 6291460
  327.1 4.8 %copy-start.1 = (bf16[2048,1024]{1,0:T(8,128)(2,1)S(1)}, bf16[2048,1024]{1,0:T(8,128)(2,1)}, u32[]{:S(2)}) copy-start(bf16[2048,1024]{1,0:T(8,128)(2,1)} %get-tuple-element.9) | copy-start | bytes 12582916
  331.9 3.7 %copy-start = (bf16[2048,1024]{1,0:T(8,128)(2,1)S(1)}, bf16[2048,1024]{1,0:T(8,128)(2,1)}, u32[]{:S(2)}) copy-start(bf16[2048,1024]{1,0:T(8,128)(2,1)} %get-tuple-element.10) | copy-start | bytes 12582916
  335.6 2.0 copy-start.3

commit v2 on v1

--- a/solution.py
+++ b/solution.py
@@ -8,14 +8,15 @@
 
 MESH = pl.DeviceIdType.MESH
 VMEM_LIMIT = 66 * 1000 * 1000
+EPSILON = 1e-05
 
 
 def kernel(ng, nz, nt, tok_in, wt, gw, uw, dw, gout, uout, dout, mixed,
            tok, hid, part, crx, yrx, ret,
-           ts, tr, fs_s, fr, ws, wr, xs, xr, cs, cr, ys, yr, rs, rr):
+           ts, tr, fs_s, fr, own, ws, wr, xs, xr, cs, cr, ys, yr, rs, rr):
     g, z, t = lax.axis_index("gr"), lax.axis_index("fs"), lax.axis_index("tp")
     core, y = lax.rem(t, 2), lax.div(t, 2)
-    rows, quarter = tok_in.shape[1], tok_in.shape[2]
+    rows, quarter = tok_in.shape[0], tok_in.shape[1] // nt
     chunk, width = gw.shape[1], gw.shape[2]
     chunks = ng * nz
     per_owner = chunks // nt
@@ -66,35 +67,81 @@
         ref = rows_of(m, 1 - g, frm(k))
         rdma(ref, ref, xs.at[m, k], xr.at[m, k], {"gr": 1 - g}).wait_recv()
 
-    for m in range(3):
-        x_send(m, 0, srcs[m].at[z])
-    for k in ks:
-        c = rdma(tok_in.at[t], tok.at[t, z], ts.at[k], tr.at[k], {"fs": to(k)})
+    x_send(0, 0, gw.at[z])
+    for k in ks:
+        z_send(0, k)
+    x_send(1, 0, uw.at[z])
+    x_send(2, 0, dw.at[z])
+    own_rows = pl.ds(pl.multiple_of((g * nz + z) * chunk, chunk), chunk)
+    own_down = pltpu.make_async_copy(dw.at[z], dout.at[own_rows, :], own)
+    own_down.start()
+
+    step = 64
+
+    @pl.loop(0, rows // step)
+    def _(i):
+        at = pl.ds(pl.multiple_of(i * step, step), step)
+        x = tok_in[at, :].astype(jnp.float32)
+        scale = lax.rsqrt(jnp.mean(x * x, axis=-1, keepdims=True) + EPSILON)
+        x = (x * scale).astype(jnp.bfloat16)
+        for q in range(nt):
+            tok[q, z, at, :] = x[:, q * quarter:(q + 1) * quarter]
+
+    for m in range(2):
+        outs[m][own_rows, :] = srcs[m][z]
+
+    guarded = []
+
+    def guard(flag, c):
+        @pl.when(flag)
+        def _():
+            c.start()
+        guarded.append((flag, c))
+
+    def hop(way, h, src):
+        nxt = lax.rem(z + way + nz, nz)
+        ref = tok.at[t, src]
+        return rdma(ref, ref, ts.at[(way + 1) // 2, h], tr.at[src], {"fs": nxt})
+
+    right, left = z + 1 < nz, z >= 1
+    guard(right, hop(1, 0, z))
+    guard(left, hop(-1, 0, z))
+    z_send(1, ks[0])
+    for k in ks:
+        z_take(0, k)
+    mate, over = y * 2 + 1 - core, (1 - y) * 2 + core
+    for h in range(1, nz):
+        for way in (1, -1):
+            src = lax.rem(z - way * h + nz, nz)
+            valid = z >= h if way == 1 else z + h < nz
+            more = right if way == 1 else left
+            ref = tok.at[t, src]
+
+            @pl.when(valid)
+            def _(ref=ref, src=src):
+                rdma(ref, ref, ts.at[0, 0], tr.at[src], {"fs": lax.rem(z + 1, nz)}).wait_recv()
+            guard(jnp.logical_and(valid, more), hop(way, h, src))
+            guard(valid, rdma(ref, ref, fs_s.at[1, src], fr.at[1, src], {"tp": over}))
+            guard(valid, rdma(ref, ref, fs_s.at[0, src], fr.at[0, src], {"tp": mate}))
+        if h < len(ks):
+            z_send(1, ks[h])
+    for k in ks:
+        z_send(2, k)
+    z_take(1, ks[0])
+    for k in ks:
+        src = frm(k)
+        ref = tok.at[over, src]
+        rdma(ref, ref, fs_s.at[1, src], fr.at[1, src], {"tp": over}).wait_recv()
+        c = rdma(ref, ref, fs_s.at[2, src], fr.at[2, src], {"tp": mate})
         c.start()
         sends.append(c)
-    for m in range(2):
-        for k in ks:
-            z_send(m, k)
-    for m in range(3):
-        outs[m][pl.ds(pl.multiple_of((g * nz + z) * chunk, chunk), chunk), :] = srcs[m][z]
-    for q in range(nt):
-        tok[q, z] = tok_in[q]
-    for k in ks:
-        ref = tok.at[t, frm(k)]
-        rdma(ref, ref, ts.at[k], tr.at[k], {"fs": to(k)}).wait_recv()
-        for j in range(1, nt):
-            c = rdma(ref, ref, fs_s.at[j, k], fr.at[j, k], {"tp": lax.rem(t + j, nt)})
-            c.start()
-            sends.append(c)
-    for k in ks:
-        z_send(2, k)
-    for m in range(2):
-        for k in ks:
-            z_take(m, k)
-    for k in ks:
-        for j in range(1, nt):
-            ref = tok.at[lax.rem(t + nt - j, nt), frm(k)]
-            rdma(ref, ref, fs_s.at[j, k], fr.at[j, k], {"tp": lax.rem(t + j, nt)}).wait_recv()
+    for k in ks[1:]:
+        z_take(1, k)
+    for k in ks:
+        src = frm(k)
+        for lane, who in ((0, mate), (2, (1 - y) * 2 + 1 - core)):
+            ref = tok.at[who, src]
+            rdma(ref, ref, fs_s.at[lane, src], fr.at[lane, src], {"tp": mate}).wait_recv()
     for m in range(2):
         for k in [0] + ks:
             x_take(m, k)
@@ -121,14 +168,15 @@
     for i, hi in enumerate(cuts):
         hidden(done, hi)
         done = hi
-        if i >= 1 and len(late) > 1:
+        if i >= 1 and late:
             z_take(2, late.pop(0))
 
     def ids(c):
         owner = c // per_owner
         return owner, lax.rem(owner, 2), lax.div(owner, 2), lax.rem(c, per_owner)
 
-    finals = []
+    own_down.wait()
+    finals = guarded
 
     def stage_a(i, c):
         mine = pl.ds(pl.multiple_of(c * chunk, chunk), chunk)
@@ -190,22 +238,20 @@
         for h in home:
             finals.append((owner == t, h))
 
-    order = [(0, 0), (1, 0)] + [(0, k) for k in ks] + [(1, k) for k in ks]
+    order = [(side, k) for k in [0] + ks for side in (0, 1)]
+    lag = 4
     seq = [((g if side == 0 else 1 - g) * nz + frm(k), side, k) for side, k in order]
     n = len(seq)
-    for i in range(n + 2):
+    for i in range(n + lag):
         if i < n:
             c, side, k = seq[i]
             if side == 1:
                 x_take(2, k)
-            elif k in late:
-                z_take(2, k)
-                late.remove(k)
             stage_a(i, c)
         if 0 <= i - 1 < n:
             stage_b(i - 1, seq[i - 1][0])
-        if 0 <= i - 2 < n:
-            stage_c(i - 2, seq[i - 2][0])
+        if 0 <= i - lag < n:
+            stage_c(i - lag, seq[i - lag][0])
 
     for k in ks:
         for cc in range(per_owner):
@@ -233,11 +279,6 @@
     experts, chunk, width = w_gate.shape
     chunks = ng * nz
     per_owner = chunks // nt
-    float_rows = tokens.astype(jnp.float32)
-    normed = (
-        float_rows * lax.rsqrt(jnp.mean(float_rows * float_rows, axis=-1, keepdims=True) + EPSILON)
-    ).astype(jnp.bfloat16)
-    normed = normed.reshape(rows, nt, quarter).transpose(1, 0, 2)
     ids = jnp.arange(experts, dtype=jnp.int32)
     wt = jnp.sum(jnp.where(routes[:, :, None] == ids, route_weight[:, :, None], 0.0), axis=1)
     bf = jnp.bfloat16
@@ -247,7 +288,7 @@
     outs = pl.pallas_call(
         functools.partial(kernel, ng, nz, nt),
         out_shape=(full, full, full, jax.ShapeDtypeStruct((rows, quarter), bf)),
-        in_specs=[vmem] * 5,
+        in_specs=[vmem] * 4 + [pl.BlockSpec(memory_space=pl.ANY)],
         out_specs=(vmem,) * 4,
         scratch_shapes=[
             pltpu.VMEM((nt, nz, rows, quarter), bf),
@@ -256,8 +297,8 @@
             pltpu.VMEM((chunks // 2, nz, rows, chunk), bf),
             pltpu.VMEM((per_owner, nz, rows, chunk), bf),
             pltpu.VMEM((nz, per_owner, rows, chunk), bf),
-            dma((nz,)), dma((nz,)),
-            dma((nt, nz)), dma((nt, nz)),
+            dma((2, nz)), dma((nz,)),
+            dma((3, nz)), dma((3, nz)), dma,
             dma((3, nz)), dma((3, nz)),
             dma((3, nz)), dma((3, nz)),
             dma((chunks,)), dma((chunks,)),
@@ -267,14 +308,11 @@
         compiler_params=pltpu.CompilerParams(
             collective_id=0, has_side_effects=True, vmem_limit_bytes=VMEM_LIMIT
         ),
-    )(normed, wt, gate_local, up_local, w_down)
+    )(tokens, wt, gate_local, up_local, w_down)
     gate_out, up_out, down_out, mixed = outs
     return (gate_out[None], up_out[None], down_out[None], mixed)
 
 EXP_DEV = 1
-
-
-EPSILON = 1e-05
 
 
 def body(tokens, routes, route_weight, gain, w_gate, w_up, w_down):

time: 339 us -> 295 us (0.87); the launches traced: 338 us -> 290 us
  Pallas kernels: 310 us -> 270 us
  local copies, waits for them, and re-layouts: 19.3 us -> 12.2 us
    pallas_call x1, Pallas kernels: 310 us -> 270 us  [fused(): pl.pallas_call(functools.partial(kernel, ng, nz, nt), out_shape=(full, fu...]
    reshape x1 -> x0, local copies, waits for them, and re-layouts: 4.28 us -> none  [fused(): normed = normed.reshape(rows, nt, quarter).transpose(1, 0, 2)]
    unnamed x15 -> x10, local copies, waits for them, and re-layouts: 14.2 us -> 11.3 us
where the time goes in v2:
time: 295 us; the launch traced here: 290 us
  Pallas kernels  270 us (92%)
  local copies, waits for them, and re-layouts  12.2 us (4%)
  other arithmetic  6.66 us (2%)
    pallas_call x1, Pallas kernels, fused(): pl.pallas_call(functools.partial(kernel, ng, nz, nt), out_shape=(full, fu...  270 us
    unnamed x10, local copies, waits for them, and re-layouts  11.3 us
    convert_element_type x1, other arithmetic, fused(): up_local = (w_up * scaling).astype(jnp.bfloat16)  5.94 us

profile of v2, /device:TPU:4, one launch (start us, length us, event | category | flops | bytes accessed | tf_op | source)
XLA Modules:
  0.0 289.8 jit_solution(8320763540453356149)
XLA Ops:
  0.6 0.7 select_reduce_fusion
  1.4 0.9 copy.13.wt
  2.2 5.9 %multiply_convert_fusion = (bf16[4,256,1024]{2,1,0:T(8,128)(2,1)}, bf16[4,256,1024]{2,1,0:T(8,128)(2,1)}) fusion(bf16[4,256,1024]{2,1,0:T(8,128)(2,1)} %param.12, f32[256]{0:T(256)} %param.10, bf16[4,256,1024]{2,1,0:T(8,128)(2,1)} %param.11), kind=kLoop, calls=%fused_computation | loop fusion | flops 6291456 | bytes 8389632 | tf_op jit(solution)/shard_map/convert_element_type | solution.py:276
  8.2 270.3 %shard_map.102 = (bf16[2048,1024]{1,0:T(8,128)(2,1)}, bf16[2048,1024]{1,0:T(8,128)(2,1)}, bf16[2048,1024]{1,0:T(8,128)(2,1)}, bf16[512,512]{1,0:T(8,128)(2,1)}) custom-call(bf16[512,2048]{1,0:T(8,128)(2,1)} %tok_in.1, f32[512,4]{1,0:T(8,128)} %copy.13.wt, bf16[4,256,1024]{2,1,0:T(8,128)(2,1)} %get-tuple-element.13.gw, ...), custom_call_target="tpu_custom_call" | custom-call | tf_op jit(solution)/shard_map/pallas_call | solution.py:288
  278.4 0.0 copy-start.1
  278.5 4.8 %copy.18 = bf16[1,2048,1024]{2,1,0:T(8,128)(2,1)} copy(bf16[1,2048,1024]{2,1,0:T(8,128)(2,1)} %bitcast.5) | data formatting | bytes 8388608
  283.3 0.0 copy-done.1
  283.3 0.0 copy-start
  283.3 2.1 copy.19
  285.4 1.6 copy-done
  287.0 0.0 copy-start.2
  287.0 2.0 copy.20
  289.0 0.0 copy-done.2
  289.0 0.8 copy.21
Async XLA Ops:
  278.4 4.8 %copy-start.1 = (bf16[2048,1024]{1,0:T(8,128)(2,1)S(1)}, bf16[2048,1024]{1,0:T(8,128)(2,1)}, u32[]{:S(2)}) copy-start(bf16[2048,1024]{1,0:T(8,128)(2,1)} %get-tuple-element.9) | copy-start | bytes 12582916
  283.3 3.7 %copy-start = (bf16[2048,1024]{1,0:T(8,128)(2,1)S(1)}, bf16[2048,1024]{1,0:T(8,128)(2,1)}, u32[]{:S(2)}) copy-start(bf16[2048,1024]{1,0:T(8,128)(2,1)} %get-tuple-element.10) | copy-start | bytes 12582916
  287.0 2.0 copy-start.2
